TPU v7x, 32 devices: a whole 2x2x4 slice. The times are simulated.
32 devices in a mesh: ep: 4 (over y, x), tp: 8 (over z, core).
Axes of the slice: x: 2, y: 2, z: 4, core: 2. Of those that a mesh axis runs over, the one named last changes fastest.
Arguments:
- tokens: bfloat16 [1024, 2048], P('ep', 'tp'), may hold values from -600 to 600
- pre_gain: float32 [2048], P('tp'), may hold values from 0.1 to 1.9
- expert_gate: bfloat16 [4, 2048, 8192], P('ep', None, 'tp'), may hold values from -0.125 to 0.125
- expert_up: bfloat16 [4, 2048, 8192], P('ep', None, 'tp'), may hold values from -0.125 to 0.125
- expert_down: bfloat16 [4, 8192, 2048], P('ep', 'tp'), may hold values from -8 to 8
- routes: int32 [1024, 2], P('ep'), may hold values from 0 to 3, all different within a row; in each aligned block of 256 rows (0 to 255, 256 to 511, ...) at most 192 rows name the same one
- route_weights: float32 [1024, 2], P('ep'), may hold values from 0.1 to 1
- post_gain: float32 [2048], P('tp'), may hold values from 0.1 to 1.9
Outputs:
- layer_out: bfloat16 [1024, 2048], P('ep', 'tp')
Inputs may be any that keep to these rules, and one draw needn't show every extreme that they name: `routes`: each token names 2 different experts. Among the 256 tokens of one index of ep no expert is named more than 192 times, a bound that some expert reaches in some of these blocks.
All inputs are finite; a program needn't handle non-finite values.
Results may differ from a plain program's by a relative error of at most 0.024.
Values may be sent and summed in bfloat16 or wider, within the bound.
A program may use at most 64 MiB of HBM per device.

v0:
```python
import jax
import jax.numpy as jnp
from jax import lax
from jax.sharding import PartitionSpec as P

EPSILON = 1e-06


def local(tokens, pre_gain, expert_gate, expert_up, expert_down, routes, route_weights, post_gain):
    local_experts = expert_gate.shape[0]
    groups = lax.axis_size("ep")
    experts_all = local_experts * groups
    tok_rows, part_width = tokens.shape
    full_width = part_width * lax.axis_size("tp")
    capacity = 3 * tok_rows // experts_all
    values = tokens.astype(jnp.float32)
    input_sq = lax.psum(jnp.sum(values * values, axis=-1), "tp")
    normed = (
        values * lax.rsqrt(input_sq / full_width + EPSILON)[:, None] * pre_gain[None, :]
    ).astype(jnp.bfloat16)
    onehot = (routes[:, :, None] == jnp.arange(experts_all, dtype=jnp.int32)).astype(jnp.int32)
    onehot = onehot.reshape(tok_rows * 2, experts_all)
    earlier = jnp.cumsum(onehot, axis=0) - onehot
    slots = jnp.sum(earlier * onehot, axis=-1).reshape(tok_rows, 2)
    positions = routes * capacity + slots
    places = jnp.arange(experts_all * capacity, dtype=jnp.int32)
    first_pick = (places[:, None] == positions[None, :, 0]).astype(jnp.bfloat16)
    second_pick = (places[:, None] == positions[None, :, 1]).astype(jnp.bfloat16)
    dispatch = first_pick + second_pick
    outgoing = jnp.dot(dispatch, normed, preferred_element_type=jnp.float32).astype(jnp.bfloat16)
    arrived = lax.all_to_all(outgoing, "ep", split_axis=0, concat_axis=0, tiled=True)
    fragment = lax.all_gather(arrived, "tp", axis=1, tiled=True)
    count = fragment.shape[1]
    grouped = fragment.reshape(groups, local_experts, capacity, count)
    gate_pre = jnp.einsum(
        "secw,ewf->secf", grouped, expert_gate, preferred_element_type=jnp.float32
    )
    up_pre = jnp.einsum("secw,ewf->secf", grouped, expert_up, preferred_element_type=jnp.float32)
    hidden = (jax.nn.silu(gate_pre) * up_pre).astype(jnp.bfloat16)
    product = jnp.einsum("secf,efd->dsec", hidden, expert_down, preferred_element_type=jnp.float32)
    summed = lax.psum_scatter(
        product.reshape(lax.axis_size("tp") * part_width, groups * local_experts * capacity).astype(
            jnp.bfloat16
        ),
        "tp",
        scatter_dimension=0,
        tiled=True,
    )
    returned = lax.all_to_all(summed, "ep", split_axis=1, concat_axis=1, tiled=True)
    contract = (((0,), (1,)), ((), ()))
    first_out = lax.dot_general(first_pick, returned, contract, preferred_element_type=jnp.float32)
    second_out = lax.dot_general(
        second_pick, returned, contract, preferred_element_type=jnp.float32
    )
    combined = route_weights[:, 0:1] * first_out + route_weights[:, 1:2] * second_out
    output_sq = lax.psum(jnp.sum(combined * combined, axis=-1), "tp")
    scaled = combined * lax.rsqrt(output_sq / full_width + EPSILON)[:, None] * post_gain[None, :]
    return scaled.astype(jnp.bfloat16)


def solution(mesh):
    placed = (
        P("ep", "tp"),
        P("tp"),
        P("ep", None, "tp"),
        P("ep", None, "tp"),
        P("ep", "tp", None),
        P("ep", None),
        P("ep", None),
        P("tp"),
    )
    return jax.shard_map(
        local, mesh=mesh, in_specs=placed, out_specs=P("ep", "tp"), check_vma=False
    )
```

profile of v0, /device:TPU:0, one launch (start us, length us, event | category | flops | bytes accessed | tf_op | source)
XLA Modules:
  0.0 164.0 jit_solution(8557718616161930768)
XLA Ops:
  6.5 0.0 all-gather.2.cloned.1.call-start
  6.5 0.8 copy.20
  7.4 0.1 eq.61
  7.5 0.1 eq.57
  7.7 1.2 reduce-window.6
  8.9 0.2 slice_reduce_fusion
  9.1 0.2 reduce-window.9
  9.3 0.1 add_bitcast_fusion
  9.4 0.1 reshape.55
  9.5 0.1 copy.22
  9.6 0.7 multiply_add_fusion
  10.3 1.0 fusion.28
  11.3 18.1 %psum.14 = f32[256]{0:T(256)S(1)} all-reduce(f32[256]{0:T(256)S(1)} %fusion.28), channel_id=1, replica_groups=mesh['ep'=4,'tp'=8] {'tp'}, use_global_device_ids=true, to_apply=%region_4.5 | all-reduce | flops 256 | bytes 2048 | tf_op jit(solution)/shard_map/psum | solution.py:17
  29.4 1.3 convolution_convert_fusion
  30.7 10.1 %all_to_all.24 = bf16[4,192,256]{2,1,0:T(8,128)(2,1)} all-to-all(bf16[4,192,256]{2,1,0:T(8,128)(2,1)S(1)} %bitcast.82), channel_id=1, replica_groups=mesh['ep'=4,'tp'=8] {'ep'}, dimensions={0} | all-to-all | bytes 786432 | tf_op jit(solution)/shard_map/all_to_all | solution.py:31
  40.8 0.0 all-gather.2.cloned.1.call-update
  40.8 0.0 reduce-scatter.2.cloned.1.call-start
  40.8 35.9 %all-gather.2.cloned.1.call-done = bf16[768,2048]{1,0:T(8,128)(2,1)} async-done(((bf16[768,256]{1,0:T(8,128)(2,1)}), bf16[768,2048]{1,0:T(8,128)(2,1)}) %all-gather.2.cloned.1.call-update) | async-done | bytes 3145744 | tf_op jit(solution)/shard_map/all_gather | solution.py:32
  76.8 6.3 %fusion.2 = f32[4,192,1024]{2,1,0:T(8,128)S(1)} fusion(bf16[4,192,2048]{2,1,0:T(8,128)(2,1)} %bitcast.90, bf16[1,2048,1024]{2,1,0:T(8,128)(2,1)} %param.11), kind=kOutput, calls=%fused_computation.2 | convolution fusion | flops 3221225472 | bytes 10485760 | tf_op jit(solution)/shard_map/secw,ewf->secf/dot_general | solution.py:38
  83.1 0.0 copy-start.3
  83.1 3.8 %fusion.9 = bf16[4,1,192,1024]{3,2,0,1:T(8,128)(2,1)S(1)} fusion(f32[4,192,1024]{2,1,0:T(8,128)S(1)} %fusion.2, bf16[4,192,2048]{2,1,0:T(8,128)(2,1)S(1)} %bitcast.91, bf16[1,2048,1024]{2,1,0:T(8,128)(2,1)S(1)} %copy-done.2), kind=kOutput, calls=%fused_computation.8 | convolution fusion | flops 3225944064 | bytes 12058624 | tf_op jit(solution)/shard_map/secw,ewf->secf/dot_general | solution.py:35
  87.0 4.8 %fusion.13 = bf16[2048,768]{0,1:T(8,128)(2,1)} fusion(bf16[768,1024]{1,0:T(8,128)(2,1)S(1)} %bitcast.92, bf16[1,1024,2048]{2,1,0:T(8,128)(2,1)S(1)} %copy-done.3), kind=kOutput, calls=%fused_computation.14 | convolution fusion | flops 3222798336 | bytes 8912896 | tf_op jit(solution)/shard_map/secf,efd->dsec/dot_general | solution.py:40
  91.8 0.0 reduce-scatter.2.cloned.1.call-update
  91.8 38.8 %reduce-scatter.2.cloned.1.call-done = bf16[256,768]{0,1:T(8,128)(2,1)} async-done(((bf16[2048,768]{0,1:T(8,128)(2,1)}), bf16[256,768]{0,1:T(8,128)(2,1)}) %reduce-scatter.2.cloned.1.call-update) | async-done | bytes 393232 | tf_op jit(solution)/shard_map/reduce_scatter | solution.py:41
  130.6 3.6 %all-to-all-start.1 = ((bf16[256,4,192]{0,2,1:T(8,128)(2,1)}), bf16[256,4,192]{0,2,1:T(8,128)(2,1)S(1)}, u32[]{:S(2)}, u32[]{:S(2)}) async-start(bf16[256,4,192]{0,2,1:T(8,128)(2,1)} %bitcast.81), calls=%async_computation.2 | async-start | bytes 786432 | tf_op jit(solution)/shard_map/all_to_all | solution.py:49
  134.2 5.9 %all-to-all-done.1 = bf16[256,4,192]{0,2,1:T(8,128)(2,1)S(1)} async-done(((bf16[256,4,192]{0,2,1:T(8,128)(2,1)}), bf16[256,4,192]{0,2,1:T(8,128)(2,1)S(1)}, u32[]{:S(2)}, u32[]{:S(2)}) %all-to-all-start.1) | async-done | bytes 393248 | tf_op jit(solution)/shard_map/all_to_all | solution.py:49
  140.1 0.4 convolution_multiply_fusion.1
  140.5 0.4 multiply_reduce_fusion
  140.9 15.4 %psum.15 = f32[256]{0:T(256)S(1)} all-reduce(f32[256]{0:T(256)S(1)} %get-tuple-element.9), channel_id=1, replica_groups=mesh['ep'=4,'tp'=8] {'tp'}, use_global_device_ids=true, to_apply=%region_7.8 | all-reduce | flops 256 | bytes 2048 | tf_op jit(solution)/shard_map/psum | solution.py:56
  156.3 0.0 copy-done.1
  156.3 0.1 multiply_convert_fusion
  156.4 0.8 copy.23
  (14 shorter events, 0.1 us)
Async XLA Ops:
  6.5 70.3 %all-gather.2.cloned.1.call-start = ((), (), s32[]{:S(2)}) async-start(), calls=%async_computation.3 | async-start | bytes 3538944 | tf_op jit(solution)/shard_map/all_gather | solution.py:32
  40.8 89.8 %reduce-scatter.2.cloned.1.call-start = ((), (), s32[]{:S(2)}) async-start(), calls=%async_computation.4 | async-start | bytes 3538944 | tf_op jit(solution)/shard_map/reduce_scatter | solution.py:41
  76.8 6.3 %copy-start.2 = (bf16[1,2048,1024]{2,1,0:T(8,128)(2,1)S(1)}, bf16[1,2048,1024]{2,1,0:T(8,128)(2,1)}, u32[]{:S(2)}) copy-start(bf16[1,2048,1024]{2,1,0:T(8,128)(2,1)} %param.10) | copy-start | bytes 12582916
  76.8 6.3 %copy-start.4 = (bf16[768,2048]{1,0:T(8,128)(2,1)S(1)}, bf16[768,2048]{1,0:T(8,128)(2,1)}, u32[]{:S(2)}) copy-start(bf16[768,2048]{1,0:T(8,128)(2,1)} %all-gather.2.cloned.1.call-done) | copy-start | bytes 9437188
  83.1 3.9 %copy-start.3 = (bf16[1,1024,2048]{2,1,0:T(8,128)(2,1)S(1)}, bf16[1,1024,2048]{2,1,0:T(8,128)(2,1)}, u32[]{:S(2)}) copy-start(bf16[1,1024,2048]{2,1,0:T(8,128)(2,1)} %param.12) | copy-start | bytes 12582916
  91.8 42.4 %copy-start = (f32[256,2]{0,1:T(2,128)S(1)}, f32[256,2]{0,1:T(2,128)}, u32[]{:S(2)}) copy-start(f32[256,2]{0,1:T(2,128)} %param.14) | copy-start | bytes 6148
  91.8 64.5 %copy-start.1 = (f32[256]{0:T(256)S(1)}, f32[256]{0:T(256)}, u32[]{:S(2)}) copy-start(f32[256]{0:T(256)} %param.15) | copy-start | bytes 3076
  130.6 9.5 %all-to-all-start.1 = ((bf16[256,4,192]{0,2,1:T(8,128)(2,1)}), bf16[256,4,192]{0,2,1:T(8,128)(2,1)S(1)}, u32[]{:S(2)}, u32[]{:S(2)}) async-start(bf16[256,4,192]{0,2,1:T(8,128)(2,1)} %bitcast.81), calls=%async_computation.2 | async-start | bytes 786432 | tf_op jit(solution)/shard_map/all_to_all | solution.py:49
Sparse Core Ops, SparseCore 0:
  40.9 35.8 all-gather.1
  91.9 38.5 reduce-scatter.1
where the time goes:
time: 164 us
  waiting for transfers between devices  80.6 us (49%)
  blocking collectives  43.6 us (27%)
  matrix products  17 us (10%)
  between operations  13.5 us (8%)
  starting transfers between devices  3.69 us (2%)
  other arithmetic  3.35 us (2%)
  local copies, waits for them, and re-layouts  2.31 us (1%)
    reduce_scatter x1, waiting for transfers between devices, local(): lax.psum_scatter(product.reshape(lax.axis_size('tp') * part_width, groups...  38.8 us
    all_gather x1, waiting for transfers between devices, local(): fragment = lax.all_gather(arrived, 'tp', axis=1, tiled=True)  35.9 us
    psum x1, blocking collectives, local(): input_sq = lax.psum(jnp.sum(values * values, axis=-1), 'tp')  18.1 us
    psum x1, blocking collectives, local(): output_sq = lax.psum(jnp.sum(combined * combined, axis=-1), 'tp')  15.4 us
    all_to_all x1, blocking collectives, local(): lax.all_to_all(outgoing, 'ep', split_axis=0, concat_axis=0, tiled=True)  10.1 us
    dot_general x1, matrix products, local(): jnp.einsum('secw,ewf->secf', grouped, expert_up, preferred_element_type=j...  6.28 us
    all_to_all x1, waiting for transfers between devices, local(): lax.all_to_all(summed, 'ep', split_axis=1, concat_axis=1, tiled=True)  5.87 us
    dot_general x1, matrix products, local(): jnp.einsum('secf,efd->dsec', hidden, expert_down, preferred_element_type=...  4.83 us
  transfers between devices with their start and end apart: 3, of which 3 were waited for; matrix products, arithmetic and copies ran while one was open for 0% of the time, Pallas kernels for 0%

commit v1 on v0

--- a/solution.py
+++ b/solution.py
@@ -29,7 +29,14 @@
     dispatch = first_pick + second_pick
     outgoing = jnp.dot(dispatch, normed, preferred_element_type=jnp.float32).astype(jnp.bfloat16)
     arrived = lax.all_to_all(outgoing, "ep", split_axis=0, concat_axis=0, tiled=True)
-    fragment = lax.all_gather(arrived, "tp", axis=1, tiled=True)
+    peers = lax.axis_size("tp")
+    right = [(i, (i + 1) % peers) for i in range(peers)]
+    parts = [arrived]
+    for far in range(1, peers):
+        parts = [lax.ppermute(parts[0], "tp", right), *parts]
+    out = jnp.concatenate(parts, axis=1)
+    places_2 = (lax.axis_index("tp") + 1) * parts[-1].shape[1]
+    fragment = jnp.roll(out, places_2, axis=1)
     count = fragment.shape[1]
     grouped = fragment.reshape(groups, local_experts, capacity, count)
     gate_pre = jnp.einsum(

time: 164 us -> 189 us (1.15)
  waiting for transfers between devices: 80.6 us -> 106 us
  matrix products: 17 us -> 13.9 us
  local copies, waits for them, and re-layouts: 2.31 us -> 4.81 us
    ppermute x0 -> x7, waiting for transfers between devices: none -> 63 us  [local(): parts = [lax.ppermute(parts[0], 'tp', right), *parts]]
    all_gather x1 -> x0, waiting for transfers between devices: 35.9 us -> none  [local(): fragment = lax.all_gather(arrived, 'tp', axis=1, tiled=True)]
    dot_general x1, matrix products: 6.28 us -> 3.6 us  [local(): jnp.einsum('secw,ewf->secf', grouped, expert_up, preferred_element_type=j...]
    unnamed x11 -> x26, local copies, waits for them, and re-layouts: 0.83 us -> 2.88 us
  transfers between devices with their start and end apart: 3 -> 9, of which waited for: 3 -> 9; matrix products, arithmetic and copies ran while one was open for 0% -> 0% of each run, Pallas kernels for 0% -> 0%
where the time goes in v1:
time: 189 us
  waiting for transfers between devices  106 us (56%)
  blocking collectives  43.5 us (23%)
  matrix products  13.9 us (7%)
  between operations  13.7 us (7%)
  local copies, waits for them, and re-layouts  4.81 us (3%)
  starting transfers between devices  3.67 us (2%)
  other arithmetic  3.35 us (2%)
    ppermute x7, waiting for transfers between devices, local(): parts = [lax.ppermute(parts[0], 'tp', right), *parts]  63 us
    reduce_scatter x1, waiting for transfers between devices, local(): lax.psum_scatter(product.reshape(lax.axis_size('tp') * part_width, groups...  37.2 us
    psum x1, blocking collectives, local(): input_sq = lax.psum(jnp.sum(values * values, axis=-1), 'tp')  18.1 us
    psum x1, blocking collectives, local(): output_sq = lax.psum(jnp.sum(combined * combined, axis=-1), 'tp')  15.4 us
    all_to_all x1, blocking collectives, local(): lax.all_to_all(outgoing, 'ep', split_axis=0, concat_axis=0, tiled=True)  9.95 us
    all_to_all x1, waiting for transfers between devices, local(): lax.all_to_all(summed, 'ep', split_axis=1, concat_axis=1, tiled=True)  5.87 us
    dot_general x1, matrix products, local(): jnp.einsum('secf,efd->dsec', hidden, expert_down, preferred_element_type=...  4.85 us
  transfers between devices with their start and end apart: 9, of which 9 were waited for; matrix products, arithmetic and copies ran while one was open for 0% of the time, Pallas kernels for 0%

profile of v1, /device:TPU:0, one launch (start us, length us, event | category | flops | bytes accessed | tf_op | source)
XLA Modules:
  0.0 188.9 jit_solution(16544853255921995644)
XLA Ops:
  6.5 0.8 copy.20
  7.4 0.1 eq.64
  7.5 0.1 eq.60
  7.7 1.2 reduce-window.6
  8.9 0.2 slice_reduce_fusion
  9.1 0.2 reduce-window.9
  9.4 0.1 reshape.55
  9.6 0.7 multiply_add_fusion
  10.3 1.0 fusion.28
  11.3 18.1 %psum.14 = f32[256]{0:T(256)S(1)} all-reduce(f32[256]{0:T(256)S(1)} %fusion.28), channel_id=1, replica_groups=mesh['ep'=4,'tp'=8] {'tp'}, use_global_device_ids=true, to_apply=%region_4.5 | all-reduce | flops 256 | bytes 2048 | tf_op jit(solution)/shard_map/psum | solution.py:17
  29.4 1.3 convolution_convert_fusion
  30.7 9.9 %all_to_all.24 = bf16[4,192,256]{2,1,0:T(8,128)(2,1)S(1)} all-to-all(bf16[4,192,256]{2,1,0:T(8,128)(2,1)S(1)} %bitcast.86), channel_id=1, replica_groups=mesh['ep'=4,'tp'=8] {'ep'}, dimensions={0} | all-to-all | bytes 786432 | tf_op jit(solution)/shard_map/all_to_all | solution.py:31
  40.7 9.0 %collective-permute-done = bf16[768,256]{1,0:T(8,128)(2,1)S(1)} collective-permute-done((bf16[768,256]{1,0:T(8,128)(2,1)S(1)}, bf16[768,256]{1,0:T(8,128)(2,1)S(1)}, u32[]{:S(2)}, u32[]{:S(2)}) %collective-permute-start) | collective-permute-done | bytes 393248 | tf_op jit(solution)/shard_map/ppermute | solution.py:36
  49.7 9.0 %collective-permute-done.1 = bf16[768,256]{1,0:T(8,128)(2,1)S(1)} collective-permute-done((bf16[768,256]{1,0:T(8,128)(2,1)S(1)}, bf16[768,256]{1,0:T(8,128)(2,1)S(1)}, u32[]{:S(2)}, u32[]{:S(2)}) %collective-permute-start.1) | collective-permute-done | bytes 393248 | tf_op jit(solution)/shard_map/ppermute | solution.py:36
  58.7 9.0 %collective-permute-done.2 = bf16[768,256]{1,0:T(8,128)(2,1)S(1)} collective-permute-done((bf16[768,256]{1,0:T(8,128)(2,1)S(1)}, bf16[768,256]{1,0:T(8,128)(2,1)S(1)}, u32[]{:S(2)}, u32[]{:S(2)}) %collective-permute-start.2) | collective-permute-done | bytes 393248 | tf_op jit(solution)/shard_map/ppermute | solution.py:36
  67.7 9.0 %collective-permute-done.3 = bf16[768,256]{1,0:T(8,128)(2,1)S(1)} collective-permute-done((bf16[768,256]{1,0:T(8,128)(2,1)S(1)}, bf16[768,256]{1,0:T(8,128)(2,1)S(1)}, u32[]{:S(2)}, u32[]{:S(2)}) %collective-permute-start.3) | collective-permute-done | bytes 393248 | tf_op jit(solution)/shard_map/ppermute | solution.py:36
  76.7 9.0 %collective-permute-done.4 = bf16[768,256]{1,0:T(8,128)(2,1)S(1)} collective-permute-done((bf16[768,256]{1,0:T(8,128)(2,1)S(1)}, bf16[768,256]{1,0:T(8,128)(2,1)S(1)}, u32[]{:S(2)}, u32[]{:S(2)}) %collective-permute-start.4) | collective-permute-done | bytes 393248 | tf_op jit(solution)/shard_map/ppermute | solution.py:36
  85.7 9.0 %collective-permute-done.5 = bf16[768,256]{1,0:T(8,128)(2,1)S(1)} collective-permute-done((bf16[768,256]{1,0:T(8,128)(2,1)S(1)}, bf16[768,256]{1,0:T(8,128)(2,1)S(1)}, u32[]{:S(2)}, u32[]{:S(2)}) %collective-permute-start.5) | collective-permute-done | bytes 393248 | tf_op jit(solution)/shard_map/ppermute | solution.py:36
  94.7 9.0 %collective-permute-done.6 = bf16[768,256]{1,0:T(8,128)(2,1)S(1)} collective-permute-done((bf16[768,256]{1,0:T(8,128)(2,1)S(1)}, bf16[768,256]{1,0:T(8,128)(2,1)S(1)}, u32[]{:S(2)}, u32[]{:S(2)}) %collective-permute-start.6) | collective-permute-done | bytes 393248 | tf_op jit(solution)/shard_map/ppermute | solution.py:36
  104.6 0.4 constant_dynamic-slice_fusion
  105.0 1.3 copy-done.2
  106.3 3.4 %fusion.4 = f32[4,192,1024]{2,1,0:T(8,128)S(1)} fusion(bf16[4,192,2048]{2,1,0:T(8,128)(2,1)S(1)} %bitcast.81, bf16[1,2048,1024]{2,1,0:T(8,128)(2,1)S(1)} %copy-done.2), kind=kOutput, calls=%fused_computation.4 | convolution fusion | flops 3221225472 | bytes 10485760 | tf_op jit(solution)/shard_map/secw,ewf->secf/dot_general | solution.py:42
  109.7 3.6 %fusion.9 = bf16[4,1,192,1024]{3,2,0,1:T(8,128)(2,1)S(1)} fusion(f32[4,192,1024]{2,1,0:T(8,128)S(1)} %fusion.4, bf16[4,192,2048]{2,1,0:T(8,128)(2,1)S(1)} %bitcast.82, bf16[1,2048,1024]{2,1,0:T(8,128)(2,1)S(1)} %copy-done.3), kind=kOutput, calls=%fused_computation.8 | convolution fusion | flops 3225944064 | bytes 12058624 | tf_op jit(solution)/shard_map/secw,ewf->secf/dot_general | solution.py:45
  113.4 4.8 %fusion.13 = bf16[2048,768]{0,1:T(8,128)(2,1)} fusion(bf16[768,1024]{1,0:T(8,128)(2,1)S(1)} %bitcast.94, bf16[1,1024,2048]{2,1,0:T(8,128)(2,1)S(1)} %copy-done.4), kind=kOutput, calls=%fused_computation.14 | convolution fusion | flops 3222798336 | bytes 8912896 | tf_op jit(solution)/shard_map/secf,efd->dsec/dot_general | solution.py:47
  118.3 37.2 %reduce-scatter.2.cloned.1.call-done = bf16[256,768]{0,1:T(8,128)(2,1)} async-done(((bf16[2048,768]{0,1:T(8,128)(2,1)}), bf16[256,768]{0,1:T(8,128)(2,1)}) %reduce-scatter.2.cloned.1.call-update) | async-done | bytes 393232 | tf_op jit(solution)/shard_map/reduce_scatter | solution.py:48
  155.4 3.6 %all-to-all-start.1 = ((bf16[256,4,192]{0,2,1:T(8,128)(2,1)}), bf16[256,4,192]{0,2,1:T(8,128)(2,1)S(1)}, u32[]{:S(2)}, u32[]{:S(2)}) async-start(bf16[256,4,192]{0,2,1:T(8,128)(2,1)} %bitcast.85), calls=%async_computation.2 | async-start | bytes 786432 | tf_op jit(solution)/shard_map/all_to_all | solution.py:56
  159.1 5.9 %all-to-all-done.1 = bf16[256,4,192]{0,2,1:T(8,128)(2,1)S(1)} async-done(((bf16[256,4,192]{0,2,1:T(8,128)(2,1)}), bf16[256,4,192]{0,2,1:T(8,128)(2,1)S(1)}, u32[]{:S(2)}, u32[]{:S(2)}) %all-to-all-start.1) | async-done | bytes 393248 | tf_op jit(solution)/shard_map/all_to_all | solution.py:56
  165.0 0.4 convolution_multiply_fusion.1
  165.3 0.4 multiply_reduce_fusion
  165.7 15.4 %psum.15 = f32[256]{0:T(256)S(1)} all-reduce(f32[256]{0:T(256)S(1)} %get-tuple-element.9), channel_id=1, replica_groups=mesh['ep'=4,'tp'=8] {'tp'}, use_global_device_ids=true, to_apply=%region_7.8 | all-reduce | flops 256 | bytes 2048 | tf_op jit(solution)/shard_map/psum | solution.py:63
  181.1 0.1 multiply_convert_fusion
  181.3 0.8 copy.23
  (42 shorter events, 1.0 us)
Async XLA Ops:
  6.5 148.9 %reduce-scatter.2.cloned.1.call-start = ((), (), s32[]{:S(2)}) async-start(), calls=%async_computation.3 | async-start | bytes 3538944 | tf_op jit(solution)/shard_map/reduce_scatter | solution.py:48
  40.7 9.0 %collective-permute-start = (bf16[768,256]{1,0:T(8,128)(2,1)S(1)}, bf16[768,256]{1,0:T(8,128)(2,1)S(1)}, u32[]{:S(2)}, u32[]{:S(2)}) collective-permute-start(bf16[768,256]{1,0:T(8,128)(2,1)S(1)} %bitcast.78), channel_id=1, source_target_pairs={{0,1},{1,2},{2,3},{3,4},{4,5},{5,6},{6,7},{7,0},{8,9},{9,10},{10,1... | collective-permute-start | bytes 1179656 | tf_op jit(solution)/shard_map/ppermute | solution.py:36
  49.7 9.0 %collective-permute-start.1 = (bf16[768,256]{1,0:T(8,128)(2,1)S(1)}, bf16[768,256]{1,0:T(8,128)(2,1)S(1)}, u32[]{:S(2)}, u32[]{:S(2)}) collective-permute-start(bf16[768,256]{1,0:T(8,128)(2,1)S(1)} %collective-permute-done), channel_id=1, source_target_pairs={{0,1},{1,2},{2,3},{3,4},{4,5},{5,6},{6,7},{7,0},{8,9},{9,10},{10,1... | collective-permute-start | bytes 1179656 | tf_op jit(solution)/shard_map/ppermute | solution.py:36
  58.7 9.0 %collective-permute-start.2 = (bf16[768,256]{1,0:T(8,128)(2,1)S(1)}, bf16[768,256]{1,0:T(8,128)(2,1)S(1)}, u32[]{:S(2)}, u32[]{:S(2)}) collective-permute-start(bf16[768,256]{1,0:T(8,128)(2,1)S(1)} %collective-permute-done.1), channel_id=1, source_target_pairs={{0,1},{1,2},{2,3},{3,4},{4,5},{5,6},{6,7},{7,0},{8,9},{9,10},{10,1... | collective-permute-start | bytes 1179656 | tf_op jit(solution)/shard_map/ppermute | solution.py:36
  67.7 9.0 %collective-permute-start.3 = (bf16[768,256]{1,0:T(8,128)(2,1)S(1)}, bf16[768,256]{1,0:T(8,128)(2,1)S(1)}, u32[]{:S(2)}, u32[]{:S(2)}) collective-permute-start(bf16[768,256]{1,0:T(8,128)(2,1)S(1)} %collective-permute-done.2), channel_id=1, source_target_pairs={{0,1},{1,2},{2,3},{3,4},{4,5},{5,6},{6,7},{7,0},{8,9},{9,10},{10,1... | collective-permute-start | bytes 1179656 | tf_op jit(solution)/shard_map/ppermute | solution.py:36
  76.7 9.0 %collective-permute-start.4 = (bf16[768,256]{1,0:T(8,128)(2,1)S(1)}, bf16[768,256]{1,0:T(8,128)(2,1)S(1)}, u32[]{:S(2)}, u32[]{:S(2)}) collective-permute-start(bf16[768,256]{1,0:T(8,128)(2,1)S(1)} %collective-permute-done.3), channel_id=1, source_target_pairs={{0,1},{1,2},{2,3},{3,4},{4,5},{5,6},{6,7},{7,0},{8,9},{9,10},{10,1... | collective-permute-start | bytes 1179656 | tf_op jit(solution)/shard_map/ppermute | solution.py:36
  85.7 9.0 %collective-permute-start.5 = (bf16[768,256]{1,0:T(8,128)(2,1)S(1)}, bf16[768,256]{1,0:T(8,128)(2,1)S(1)}, u32[]{:S(2)}, u32[]{:S(2)}) collective-permute-start(bf16[768,256]{1,0:T(8,128)(2,1)S(1)} %collective-permute-done.4), channel_id=1, source_target_pairs={{0,1},{1,2},{2,3},{3,4},{4,5},{5,6},{6,7},{7,0},{8,9},{9,10},{10,1... | collective-permute-start | bytes 1179656 | tf_op jit(solution)/shard_map/ppermute | solution.py:36
  94.7 9.0 %collective-permute-start.6 = (bf16[768,256]{1,0:T(8,128)(2,1)S(1)}, bf16[768,256]{1,0:T(8,128)(2,1)S(1)}, u32[]{:S(2)}, u32[]{:S(2)}) collective-permute-start(bf16[768,256]{1,0:T(8,128)(2,1)S(1)} %collective-permute-done.5), channel_id=1, source_target_pairs={{0,1},{1,2},{2,3},{3,4},{4,5},{5,6},{6,7},{7,0},{8,9},{9,10},{10,1... | collective-permute-start | bytes 1179656 | tf_op jit(solution)/shard_map/ppermute | solution.py:36
  104.1 2.2 %copy-start.2 = (bf16[1,2048,1024]{2,1,0:T(8,128)(2,1)S(1)}, bf16[1,2048,1024]{2,1,0:T(8,128)(2,1)}, u32[]{:S(2)}) copy-start(bf16[1,2048,1024]{2,1,0:T(8,128)(2,1)} %param.10) | copy-start | bytes 12582916
  106.3 3.4 %copy-start.3 = (bf16[1,2048,1024]{2,1,0:T(8,128)(2,1)S(1)}, bf16[1,2048,1024]{2,1,0:T(8,128)(2,1)}, u32[]{:S(2)}) copy-start(bf16[1,2048,1024]{2,1,0:T(8,128)(2,1)} %param.11) | copy-start | bytes 12582916
  109.7 3.6 %copy-start.4 = (bf16[1,1024,2048]{2,1,0:T(8,128)(2,1)S(1)}, bf16[1,1024,2048]{2,1,0:T(8,128)(2,1)}, u32[]{:S(2)}) copy-start(bf16[1,1024,2048]{2,1,0:T(8,128)(2,1)} %param.12) | copy-start | bytes 12582916
  113.4 45.7 %copy-start = (f32[256,2]{0,1:T(2,128)S(1)}, f32[256,2]{0,1:T(2,128)}, u32[]{:S(2)}) copy-start(f32[256,2]{0,1:T(2,128)} %param.14) | copy-start | bytes 6148
  113.4 67.8 %copy-start.1 = (f32[256]{0:T(256)S(1)}, f32[256]{0:T(256)}, u32[]{:S(2)}) copy-start(f32[256]{0:T(256)} %param.15) | copy-start | bytes 3076
  155.4 9.5 %all-to-all-start.1 = ((bf16[256,4,192]{0,2,1:T(8,128)(2,1)}), bf16[256,4,192]{0,2,1:T(8,128)(2,1)S(1)}, u32[]{:S(2)}, u32[]{:S(2)}) async-start(bf16[256,4,192]{0,2,1:T(8,128)(2,1)} %bitcast.85), calls=%async_computation.2 | async-start | bytes 786432 | tf_op jit(solution)/shard_map/all_to_all | solution.py:56
Sparse Core Ops, SparseCore 0:
  118.4 37.0 reduce-scatter.1
